TPU v7x, 32 devices: a whole 2x2x4 slice. The times are simulated.
32 devices in a mesh: sp: 4 (over z), tp: 8 (over y, x, core).
Axes of the slice: x: 2, y: 2, z: 4, core: 2. Of those that a mesh axis runs over, the one named last changes fastest.
Arguments:
- context_activations: bfloat16 [2, 1024, 4096], P(None, 'sp', 'tp'), may hold values from -6 to 6
- first_generated_activation: bfloat16 [2, 4096], replicated, may hold values from -6 to 6
- address_projection: bfloat16 [4096, 1024], P(None, 'tp'), may hold values from -0.09375 to 0.09375
- payload_projection: bfloat16 [4096, 1024], P(None, 'tp'), may hold values from -0.09375 to 0.09375
- lookup_projection: bfloat16 [4096, 1024], P(None, 'tp'), may hold values from -0.09375 to 0.09375
- exit_gating_projection: bfloat16 [4096, 1024], P(None, 'tp'), may hold values from -0.09375 to 0.09375
- writing_intensity_projection: bfloat16 [4096, 8], replicated, may hold values from -0.09375 to 0.09375
- fading_projection: bfloat16 [4096, 8], replicated, may hold values from -0.09375 to 0.09375
- channel_fading_speed: float32 [8], replicated, may hold values from 0 to 1, as said below
- extra_fading_log: float32 [2, 1024, 8], P(None, 'sp', 'tp'), may hold values from -1 to 0, as said below
- readout_normalizer_gain: float32 [128], replicated, may hold values from 0.1 to 1.9
- exit_projection: bfloat16 [1024, 4096], P('tp'), may hold values from -0.1875 to 0.1875
Outputs:
- state_cache: bfloat16 [2, 4, 8, 128, 128], P(None, 'sp', 'tp')
- step_out: bfloat16 [2, 4096], P(None, 'tp')
Inputs may be any that keep to these rules, and one draw needn't show every extreme that they name: `channel_fading_speed`: positive rates, one a head. `extra_fading_log`: zero at all but a few positions of each prompt and head, negative there.
All inputs are finite; a program needn't handle non-finite values.
Results may differ from a plain program's by a relative error of at most 0.012.
Values may be sent and summed in bfloat16 or wider, within the bound.
A program may use at most 64 MiB of HBM per device.

v0:
```python
import jax
import jax.numpy as jnp
from jax import lax
from jax.sharding import PartitionSpec as P

BLOCK = 64
norm_eps = 1e-06
highest = lax.Precision.HIGHEST


def carried_in(value, axis, combine, identity):
    devices, position = (lax.axis_size(axis), lax.axis_index(axis))
    everything = jax.tree.map(
        lambda part, kind: lax.all_gather(part.astype(kind), axis),
        value,
        (jnp.bfloat16, jnp.bfloat16),
    )
    start = jax.tree.map(
        lambda part, zero: jnp.broadcast_to(jnp.asarray(zero, part.dtype), part.shape),
        value,
        identity,
    )

    def lap(k, before):
        reached = k < position
        new = combine(
            before, jax.tree.map(lambda part, own: part[k].astype(own.dtype), everything, value)
        )
        return jax.tree.map(lambda a, b: jnp.where(reached, a, b), new, before)

    return lax.fori_loop(0, devices, lap, start)


def carried_in_2(value, axis, combine, identity):
    devices, position = (lax.axis_size(axis), lax.axis_index(axis))
    everything = lax.all_gather(value, axis)
    start = jnp.broadcast_to(jnp.asarray(identity, value.dtype), value.shape)

    def lap(k, before):
        at = devices - 1 - k
        reached = at > position
        new = combine(before, everything[at])
        return jnp.where(reached, new, before)

    return lax.fori_loop(0, devices, lap, start)


def unit_rows(values_in):
    return values_in * lax.rsqrt(jnp.sum(values_in * values_in, axis=-1, keepdims=True) + norm_eps)


def compose(left, right):
    return jnp.einsum("...ij,...jk->...ik", left, right, precision=highest)


def segment_map(keys_in, values_in, beta_gate, fading_exponent):
    blocks = keys_in.shape[0] // BLOCK
    key_blocks = keys_in.reshape(blocks, BLOCK, -1)
    value_blocks = values_in.reshape(blocks, BLOCK, -1)
    beta_blocks = beta_gate.reshape(blocks, BLOCK)
    cumul = jnp.cumsum(fading_exponent.reshape(blocks, BLOCK), axis=-1)
    causal = jnp.tril(jnp.ones((BLOCK, BLOCK), bool))
    strict = jnp.tril(jnp.ones((BLOCK, BLOCK), bool), -1)
    gaps_log = cumul[:, :, None] - cumul[:, None, :]
    within = jnp.where(causal, jnp.exp(jnp.where(causal, gaps_log, 0.0)), 0.0)
    keys_beta = key_blocks * beta_blocks[..., None]
    strict_part = jnp.where(
        strict, jnp.einsum("nid,njd->nij", keys_beta, key_blocks, precision=highest) * within, 0.0
    )
    targets = jnp.concatenate(
        [value_blocks * beta_blocks[..., None], keys_beta * jnp.exp(cumul)[..., None]], axis=-1
    )
    system = jnp.eye(BLOCK, dtype=jnp.float32) + strict_part
    solved = lax.linalg.triangular_solve(system, targets, left_side=True, lower=True)
    width_v = value_blocks.shape[-1]
    width_k = key_blocks.shape[-1]
    pseudo_values = solved[..., :width_v]
    decayed_keys = solved[..., width_v:]
    carried_values = jnp.concatenate(
        [jnp.zeros((blocks, BLOCK, width_k), jnp.float32), pseudo_values], axis=-1
    )
    trailing = key_blocks * jnp.exp(cumul[:, -1:] - cumul)[..., None]
    block_decay = jnp.exp(cumul[:, -1])

    def advance(memory, inputs):
        pseudo, decayed, trail_keys, shrink = inputs
        fresh_values = pseudo - jnp.dot(decayed, memory, precision=highest)
        memory = memory * shrink + jnp.dot(trail_keys.T, fresh_values, precision=highest)
        return (memory, None)

    start_map = jnp.concatenate(
        [jnp.eye(width_k, dtype=jnp.float32), jnp.zeros((width_k, width_v), jnp.float32)], axis=1
    )
    memory, _ = lax.scan(advance, start_map, (carried_values, decayed_keys, trailing, block_decay))
    return memory


def combine_maps(earlier, later):
    return (compose(later[0], earlier[0]), compose(later[0], earlier[1]) + later[1])


def body(
    context_activations,
    first_generated_activation,
    address_projection,
    payload_projection,
    lookup_projection,
    exit_gating_projection,
    writing_intensity_projection,
    fading_projection,
    channel_fading_speed,
    extra_fading_log,
    readout_normalizer_gain,
    exit_projection,
):
    head_size = readout_normalizer_gain.shape[0]
    current_heads = address_projection.shape[1] // head_size
    first_head = lax.axis_index("tp") * current_heads
    beta_cols = lax.dynamic_slice_in_dim(writing_intensity_projection, first_head, current_heads, 1)
    decay_cols = lax.dynamic_slice_in_dim(fading_projection, first_head, current_heads, 1)
    logit_weight = jnp.concatenate([beta_cols, decay_cols], axis=1)
    fading_speeds = lax.dynamic_slice_in_dim(channel_fading_speed, first_head, current_heads, 0)
    seq_count, length = (context_activations.shape[0], context_activations.shape[1])
    portion = lax.all_gather(context_activations, "tp", axis=2, tiled=True)
    key_sum = jnp.einsum(
        "abf,fc->abc", portion, address_projection, preferred_element_type=jnp.float32
    )
    value_sum = jnp.einsum(
        "abf,fc->abc", portion, payload_projection, preferred_element_type=jnp.float32
    )
    logit_sum = jnp.einsum("abf,fc->abc", portion, logit_weight, preferred_element_type=jnp.float32)
    shaped = (seq_count, length, current_heads, head_size)
    keys_here = unit_rows(jax.nn.silu(key_sum).reshape(shaped)).astype(jnp.bfloat16)
    values_here = jax.nn.silu(value_sum).reshape(shaped).astype(jnp.bfloat16)
    current_scores = logit_sum.astype(jnp.bfloat16)
    beta_gate = jax.nn.sigmoid(current_scores[..., :current_heads].astype(jnp.float32))
    fading_exponent = extra_fading_log - fading_speeds * jax.nn.softplus(
        current_scores[..., current_heads:].astype(jnp.float32)
    )
    maps = jax.vmap(jax.vmap(segment_map, in_axes=(1, 1, 1, 1)))(
        keys_here.astype(jnp.float32), values_here.astype(jnp.float32), beta_gate, fading_exponent
    )
    own_moves = maps[..., :head_size]
    own_offset = maps[..., head_size:]
    heads_shape = (seq_count, current_heads, head_size)
    new_keys = unit_rows(
        jax.nn.silu(
            jnp.dot(
                first_generated_activation, address_projection, preferred_element_type=jnp.float32
            )
        ).reshape(heads_shape)
    )
    new_values = jax.nn.silu(
        jnp.dot(first_generated_activation, payload_projection, preferred_element_type=jnp.float32)
    ).reshape(heads_shape)
    new_queries = unit_rows(
        jax.nn.silu(
            jnp.dot(
                first_generated_activation, lookup_projection, preferred_element_type=jnp.float32
            )
        ).reshape(heads_shape)
    )
    out_gate = jax.nn.silu(
        jnp.dot(
            first_generated_activation, exit_gating_projection, preferred_element_type=jnp.float32
        )
    ).reshape(heads_shape)
    new_logits = jnp.dot(
        first_generated_activation, logit_weight, preferred_element_type=jnp.float32
    )
    new_beta = jax.nn.sigmoid(new_logits[:, :current_heads])
    new_decay = jnp.exp(-fading_speeds * jax.nn.softplus(new_logits[:, current_heads:]))
    intersection_kq = jnp.sum(new_keys * new_queries, axis=-1, keepdims=True)
    carried_query = new_decay[..., None] * (
        new_queries - new_beta[..., None] * new_keys * intersection_kq
    )
    own_write = new_beta[..., None] * new_values * intersection_kq
    identity = jnp.broadcast_to(jnp.eye(head_size, dtype=jnp.float32), own_moves.shape)
    prefix_moves, prefix_offset = carried_in(
        (own_moves, own_offset), "sp", combine_maps, (identity, jnp.zeros_like(own_offset))
    )
    states_here = compose(own_moves, prefix_offset) + own_offset

    def chain_later(earlier, later):
        return compose(earlier, later)

    later_moves = carried_in_2(own_moves, "sp", chain_later, identity)
    lifted = jnp.einsum("shjk,shj->shk", later_moves, carried_query, precision=highest)
    term = jnp.einsum("shk,shkv->shv", lifted, own_offset, precision=highest)
    read = lax.psum(term, "sp") + own_write
    state_cache = states_here.astype(jnp.bfloat16)[:, None]
    normed = (
        read
        * lax.rsqrt(jnp.mean(read * read, axis=-1, keepdims=True) + norm_eps)
        * readout_normalizer_gain
        * out_gate
    )
    normed = normed.astype(jnp.bfloat16).reshape(seq_count, current_heads * head_size)
    partial_out = jnp.dot(normed, exit_projection, preferred_element_type=jnp.float32)
    step_out = lax.psum_scatter(partial_out, "tp", scatter_dimension=1, tiled=True).astype(
        jnp.bfloat16
    )
    return (state_cache, step_out)


def solution(mesh):
    placed = (
        P(None, "sp", "tp"),
        P(),
        P(None, "tp"),
        P(None, "tp"),
        P(None, "tp"),
        P(None, "tp"),
        P(),
        P(),
        P(),
        P(None, "sp", "tp"),
        P(),
        P("tp", None),
    )
    return jax.shard_map(
        body,
        mesh=mesh,
        in_specs=placed,
        out_specs=(P(None, "sp", "tp", None, None), P(None, "tp")),
        check_vma=False,
    )
```

profile of v0, /device:TPU:0, one launch (start us, length us, event | category | flops | bytes accessed | tf_op | source)
XLA Modules:
  0.0 188.7 jit_solution(4630512967896987474)
XLA Ops:
  7.2 0.0 copy-start
  7.2 0.0 all-gather.5.cloned.1.call-start
  7.2 0.7 all-gather.5.cloned.1.call-update
  7.9 0.0 reduce-scatter.4.cloned.1.call-start
  8.0 0.1 copy.65
  8.1 1.3 dynamic_slice.48
  10.2 1.6 multiply_reduce_fusion.4
  11.8 1.1 multiply_reduce_fusion.3
  12.9 0.2 multiply_reduce_fusion.2
  13.1 0.9 constant_dynamic-slice_fusion.1
  14.0 0.9 convolution_bitcast_fusion.6
  14.9 0.1 subtract_multiply_fusion
  15.0 0.1 iota_compare_fusion.1
  15.1 34.9 %all-gather.5.cloned.1.call-done = bf16[2,256,4096]{2,1,0:T(8,128)(2,1)} async-done(((bf16[2,256,512]{2,1,0:T(8,128)(2,1)}), bf16[2,256,4096]{2,1,0:T(8,128)(2,1)}) %all-gather.5.cloned.1.call-update) | async-done | bytes 4194320 | tf_op jit(solution)/shard_map/all_gather | solution.py:124
  50.0 3.4 %fusion.31 = bf16[2,256,2]{1,2,0:T(2,128)(2,1)S(1)} fusion(bf16[2,256,4096]{2,1,0:T(8,128)(2,1)} %all-gather.5.cloned.1.call-done, bf16[4096,1]{0,1:T(2,128)(2,1)S(1)} %get-tuple-element.365, bf16[4096,1]{0,1:T(2,128)(2,1)S(1)} %get-tuple-element.366), kind=kOutput, calls=%fused_computation.41 | convolution fusion | flops 8422400 | bytes 4212736 | tf_op jit(solution)/shard_map/abf,fc->abc/dot_general | solution.py:131
  53.3 0.7 fusion.63
  54.1 0.0 copy-start.5
  54.1 0.1 transpose.61
  54.2 0.5 reduce_window_sum.11
  54.7 0.2 slice_reduce_fusion
  54.8 0.1 bitcast_exponential_fusion
  54.9 0.1 mul.245
  55.0 3.6 %multiply_reduce_fusion = (f32[2,256]{1,0:T(2,128)S(1)}, f32[2,256,128]{2,1,0:T(8,128)S(1)}) fusion(bf16[2,256,4096]{2,1,0:T(8,128)(2,1)} %all-gather.5.cloned.1.call-done, bf16[4096,128]{1,0:T(8,128)(2,1)S(1)} %copy-done), kind=kOutput, calls=%fused_computation.60 | convolution fusion | flops 537263616 | bytes 5507072 | tf_op jit(solution)/shard_map/abf,fc->abc/dot_general | solution.py:125
  58.5 0.1 fusion.73
  58.7 0.4 fusion.27
  59.1 39.3 %custom-call.3 = f32[2,1,4,1,64,64]{4,5,3,2,1,0:T(8,128)S(1)} custom-call(f32[2,1,4,1,64,64]{5,4,3,2,1,0:T(8,128)S(1)} %fusion.27), custom_call_target="InvertDiagBlocksLowerTriangular" | custom-call | tf_op jit(solution)/shard_map/vmap(vmap())/triangular_solve | solution.py:74
  98.4 0.0 copy-done.5
  98.5 3.5 %multiply_convert_fusion = bf16[2,256,128]{2,1,0:T(8,128)(2,1)S(1)} fusion(bf16[2,256,4096]{2,1,0:T(8,128)(2,1)} %all-gather.5.cloned.1.call-done, bf16[4096,128]{1,0:T(8,128)(2,1)S(1)} %copy-done.5), kind=kOutput, calls=%fused_computation.56 | convolution fusion | flops 537198592 | bytes 5373952 | tf_op jit(solution)/shard_map/abf,fc->abc/dot_general | solution.py:128
  101.9 0.3 multiply_multiply_fusion
  102.2 0.7 convolution_bitcast_fusion.3
  103.0 0.1 copy.42
  103.1 3.0 %while.39 = (s32[]{:T(128)}, f32[2,1,128,256]{3,2,0,1:T(8,128)S(1)}, f32[4,2,1]{1,2,0:T(1,128)S(1)}, f32[4,2,1,64,128]{4,3,0,1,2:T(8,128)S(1)}, f32[4,2,1,64,256...) while((s32[]{:T(128)}, f32[2,1,128,256]{3,2,0,1:T(8,128)S(1)}, ...), condition=%wide.region_3.4_spmd, body=%wide.region_2.3_spmd.sunk | while | flops 100827136 | bytes 1312357 | solution.py:94
  103.1 0.3 convolution_subtract_fusion.2
  103.4 0.4 fusion.110
  103.8 0.3 convolution_subtract_fusion.2
  104.1 0.4 fusion.110
  104.6 0.3 convolution_subtract_fusion.2
  104.9 0.4 fusion.110
  105.3 0.3 convolution_subtract_fusion.2
  105.6 0.4 fusion.110
  106.1 0.0 copy-start.2
  106.1 0.0 copy-start.1
  106.2 16.2 %all-gather.2 = f32[8,1,128,128]{3,2,1,0:T(8,128)S(1)} all-gather(f32[2,1,128,128]{3,2,1,0:T(8,128)S(1)} %slice_bitcast_fusion.1), channel_id=4, replica_groups=mesh['sp'=4,'tp'=8] {'sp'}, dimensions={0}, use_global_device_ids=true | all-gather | bytes 655360 | tf_op jit(solution)/shard_map/all_gather | solution.py:36
  122.4 1.8 while.40
  122.4 0.4 fusion.113
  122.9 0.4 fusion.113
  123.3 0.4 fusion.113
  123.8 0.4 fusion.113
  124.2 0.3 convolution_bitcast_fusion.5
  124.5 0.2 fusion.44
  124.7 12.1 %psum.7 = f32[2,1,128]{2,0,1:T(2,128)S(1)} all-reduce(f32[2,1,128]{2,0,1:T(2,128)S(1)} %bitcast.222), channel_id=1, replica_groups=mesh['sp'=4,'tp'=8] {'sp'}, use_global_device_ids=true, to_apply=%region_11.12 | all-reduce | flops 256 | bytes 2048 | tf_op jit(solution)/shard_map/psum | solution.py:190
  136.8 1.6 multiply_reduce_fusion.1
  138.5 3.3 %convolution_bitcast_fusion.2 = f32[4096,2]{1,0:T(8,128)} fusion(bf16[128,4096]{1,0:T(8,128)(2,1)S(1)} %copy-done.1, f32[2,1,128]{2,0,1:T(2,128)S(1)} %get-tuple-element.345, f32[128]{0:T(128)S(1)} %copy-done.4, f32[2]{0:T(128)S(1)} %add_rsqrt_fusion.1, bf16[2,4096]{1,0:T(2,128)(2,1)S(1)} %copy-done.2, bf16[4096,128]{1,0:T(8,128)(2,1)} %param.23), kind=kOutput, calls=%fused_computation.29 | convolution fusion | flops 4196352 | bytes 2147848
  141.8 0.0 reduce-scatter.4.cloned.1.call-update
  141.8 14.4 %all-gather = bf16[8,1,128,128]{3,2,1,0:T(8,128)(2,1)S(1)} all-gather(bf16[2,1,128,128]{3,2,1,0:T(8,128)(2,1)S(1)} %get-tuple-element.355), channel_id=2, replica_groups=mesh['sp'=4,'tp'=8] {'sp'}, dimensions={0}, use_global_device_ids=true | all-gather | bytes 327680 | tf_op jit(solution)/shard_map/all_gather | solution.py:14
  156.2 13.8 %all-gather.1 = bf16[8,1,128,128]{3,2,1,0:T(8,128)(2,1)S(1)} all-gather(bf16[2,1,128,128]{3,2,1,0:T(8,128)(2,1)S(1)} %get-tuple-element.354), channel_id=3, replica_groups=mesh['sp'=4,'tp'=8] {'sp'}, dimensions={0}, use_global_device_ids=true | all-gather | bytes 327680 | tf_op jit(solution)/shard_map/all_gather | solution.py:14
  170.0 1.1 while.41
  170.0 0.2 fusion.116
  170.3 0.2 fusion.116
  170.6 0.2 fusion.116
  170.8 0.2 fusion.116
  171.1 0.9 fusion.30
  172.0 8.3 %reduce-scatter.4.cloned.1.call-done = f32[512,2]{1,0:T(8,128)} async-done(((f32[4096,2]{1,0:T(8,128)}), f32[512,2]{1,0:T(8,128)}) %reduce-scatter.4.cloned.1.call-update) | async-done | bytes 4112
  180.3 1.6 copy.60
  (34 shorter events, 0.3 us)
Async XLA Ops:
  7.2 4.6 %copy-start = (bf16[4096,128]{1,0:T(8,128)(2,1)S(1)}, bf16[4096,128]{1,0:T(8,128)(2,1)}, u32[]{:S(2)}) copy-start(bf16[4096,128]{1,0:T(8,128)(2,1)} %param.20) | copy-start | bytes 3145732
  7.2 46.2 %copy-start.3 = (f32[2,256,1]{1,2,0:T(1,128)S(1)}, f32[2,256,1]{1,2,0:T(1,128)}, u32[]{:S(2)}) copy-start(f32[2,256,1]{1,2,0:T(1,128)} %param.27) | copy-start | bytes 6148
  7.2 42.8 %all-gather.5.cloned.1.call-start = ((), (), s32[]{:S(2)}) async-start(), calls=%async_computation.1 | async-start | bytes 4718592 | tf_op jit(solution)/shard_map/all_gather | solution.py:124
  7.9 172.3 %reduce-scatter.4.cloned.1.call-start = ((), (), s32[]{:S(2)}) async-start(), calls=%async_computation.2 | async-start | bytes 2359296
  54.1 44.4 %copy-start.5 = (bf16[4096,128]{1,0:T(8,128)(2,1)S(1)}, bf16[4096,128]{1,0:T(8,128)(2,1)}, u32[]{:S(2)}) copy-start(bf16[4096,128]{1,0:T(8,128)(2,1)} %param.21) | copy-start | bytes 3145732
  106.1 30.8 %copy-start.2 = (bf16[2,4096]{1,0:T(2,128)(2,1)S(1)}, bf16[2,4096]{1,0:T(2,128)(2,1)}, u32[]{:S(2)}) copy-start(bf16[2,4096]{1,0:T(2,128)(2,1)} %param.19) | copy-start | bytes 49156
  106.1 32.4 %copy-start.1 = (bf16[128,4096]{1,0:T(8,128)(2,1)S(1)}, bf16[128,4096]{1,0:T(8,128)(2,1)}, u32[]{:S(2)}) copy-start(bf16[128,4096]{1,0:T(8,128)(2,1)} %param.29) | copy-start | bytes 3145732
  106.1 32.4 %copy-start.4 = (f32[128]{0:T(128)S(1)}, f32[128]{0:T(128)}, u32[]{:S(2)}) copy-start(f32[128]{0:T(128)} %param.28) | copy-start | bytes 1540
Sparse Core Ops, SparseCore 0:
  9.9 40.0 all-gather.4
  141.9 38.3 reduce-scatter.3
where the time goes:
time: 189 us
  blocking collectives  56.6 us (30%)
  waiting for transfers between devices  43.9 us (23%)
  other arithmetic  41.5 us (22%)
  matrix products  26.6 us (14%)
  between operations  15 us (8%)
  local copies, waits for them, and re-layouts  4.71 us (2%)
    another operation x1, other arithmetic, segment_map(): lax.linalg.triangular_solve(system, targets, left_side=True, lower=True)  39.3 us
    all_gather x1, waiting for transfers between devices, body(): portion = lax.all_gather(context_activations, 'tp', axis=2, tiled=True)  34.9 us
    all_gather x2, blocking collectives, carried_in(): lax.all_gather(part.astype(kind), axis)  28.2 us
    all_gather x1, blocking collectives, carried_in_2(): everything = lax.all_gather(value, axis)  16.2 us
    psum x1, blocking collectives, body(): read = lax.psum(term, 'sp') + own_write  12.1 us
    unnamed x3, waiting for transfers between devices  8.97 us
  transfers between devices with their start and end apart: 2, of which 2 were waited for; matrix products, arithmetic and copies ran while one was open for 4% of the time, Pallas kernels for 0%

commit v1 on v0

--- a/solution.py
+++ b/solution.py
@@ -113,6 +113,11 @@
     readout_normalizer_gain,
     exit_projection,
 ):
+
+    def spread_page_all(values):
+        s_next = lax.all_gather(values, "tp")
+        return jnp.concatenate(s_next, axis=2)
+
     head_size = readout_normalizer_gain.shape[0]
     current_heads = address_projection.shape[1] // head_size
     first_head = lax.axis_index("tp") * current_heads
@@ -121,7 +126,7 @@
     logit_weight = jnp.concatenate([beta_cols, decay_cols], axis=1)
     fading_speeds = lax.dynamic_slice_in_dim(channel_fading_speed, first_head, current_heads, 0)
     seq_count, length = (context_activations.shape[0], context_activations.shape[1])
-    portion = lax.all_gather(context_activations, "tp", axis=2, tiled=True)
+    portion = spread_page_all(context_activations)
     key_sum = jnp.einsum(
         "abf,fc->abc", portion, address_projection, preferred_element_type=jnp.float32
     )

time: 189 us -> 230 us (1.22)
  waiting for transfers between devices: 43.9 us -> 72.6 us
  local copies, waits for them, and re-layouts: 4.71 us -> 18.5 us
    unnamed x3, waiting for transfers between devices: 8.97 us -> 38.3 us
    reshape x0 -> x1, local copies, waits for them, and re-layouts: none -> 7.41 us  [spread_page_all(): return jnp.concatenate(s_next, axis=2)]
    all_gather x0 -> x1, local copies, waits for them, and re-layouts: none -> 6.5 us  [spread_page_all(): s_next = lax.all_gather(values, 'tp')]
  transfers between devices with their start and end apart: 2 -> 2, of which waited for: 2 -> 2; matrix products, arithmetic and copies ran while one was open for 4% -> 3% of each run, Pallas kernels for 0% -> 0%
where the time goes in v1:
time: 230 us; the launch traced here: 229 us
  waiting for transfers between devices  72.6 us (32%)
  blocking collectives  56.7 us (25%)
  other arithmetic  41.3 us (18%)
  matrix products  24.9 us (11%)
  local copies, waits for them, and re-layouts  18.5 us (8%)
  between operations  14.9 us (6%)
    another operation x1, other arithmetic, segment_map(): lax.linalg.triangular_solve(system, targets, left_side=True, lower=True)  39.3 us
    unnamed x3, waiting for transfers between devices  38.3 us
    all_gather x1, waiting for transfers between devices, spread_page_all(): s_next = lax.all_gather(values, 'tp')  34.3 us
    all_gather x2, blocking collectives, carried_in(): lax.all_gather(part.astype(kind), axis)  28.6 us
    all_gather x1, blocking collectives, carried_in_2(): everything = lax.all_gather(value, axis)  16 us
    psum x1, blocking collectives, body(): read = lax.psum(term, 'sp') + own_write  12.1 us
    reshape x1, local copies, waits for them, and re-layouts, spread_page_all(): return jnp.concatenate(s_next, axis=2)  7.41 us
    all_gather x1, local copies, waits for them, and re-layouts, spread_page_all(): s_next = lax.all_gather(values, 'tp')  6.5 us
  transfers between devices with their start and end apart: 2, of which 2 were waited for; matrix products, arithmetic and copies ran while one was open for 3% of the time, Pallas kernels for 0%

profile of v1, /device:TPU:0, one launch (start us, length us, event | category | flops | bytes accessed | tf_op | source)
XLA Modules:
  0.0 229.4 jit_solution(9054388824659149136)
XLA Ops:
  7.2 0.0 copy-start
  7.2 0.0 all-gather.6.cloned.1.call-start
  7.2 0.7 all-gather.6.cloned.1.call-update
  7.9 0.0 reduce-scatter.4.cloned.1.call-start
  8.0 1.2 dynamic_slice.48
  9.8 0.1 copy.68
  10.0 1.6 multiply_reduce_fusion.4
  11.6 0.0 copy-done
  11.6 1.1 multiply_reduce_fusion.3
  12.7 0.2 multiply_reduce_fusion.2
  12.9 0.9 constant_dynamic-slice_fusion.1
  13.8 0.9 convolution_bitcast_fusion.6
  14.7 0.1 subtract_multiply_fusion
  14.8 0.1 iota_compare_fusion.1
  14.9 34.3 %all-gather.6.cloned.1.call-done = bf16[16,256,512]{2,1,0:T(8,128)(2,1)} async-done(((bf16[2,256,512]{2,1,0:T(8,128)(2,1)}), bf16[16,256,512]{2,1,0:T(8,128)(2,1)}) %all-gather.6.cloned.1.call-update) | async-done | bytes 4194320 | tf_op jit(solution)/shard_map/all_gather | solution.py:118
  49.2 6.5 %copy.70 = bf16[8,2,256,512]{3,0,2,1:T(8,128)(2,1)} copy(bf16[8,2,256,512]{3,2,1,0:T(8,128)(2,1)} %bitcast.219) | data formatting | bytes 8388608 | tf_op jit(solution)/shard_map/all_gather | solution.py:118
  55.7 7.4 %reshape.321 = bf16[2,256,4096]{2,1,0:T(8,128)(2,1)} reshape(bf16[2,256,8,512]{3,2,1,0:T(8,128)(2,1)} %bitcast.218) | data formatting | bytes 8388608 | tf_op jit(solution)/shard_map/reshape | solution.py:119
  63.1 3.5 %fusion.31 = bf16[2,256,2]{1,2,0:T(2,128)(2,1)S(1)} fusion(bf16[2,256,4096]{2,1,0:T(8,128)(2,1)} %reshape.321, bf16[4096,1]{0,1:T(2,128)(2,1)S(1)} %get-tuple-element.365, bf16[4096,1]{0,1:T(2,128)(2,1)S(1)} %get-tuple-element.366), kind=kOutput, calls=%fused_computation.42 | convolution fusion | flops 8422400 | bytes 4212736 | tf_op jit(solution)/shard_map/abf,fc->abc/dot_general | solution.py:136
  66.7 1.4 multiply_reduce_fusion
  68.0 0.6 fusion.63
  68.7 0.1 mul.245
  68.7 0.1 transpose.61
  68.8 0.5 reduce_window_sum.11
  69.3 0.2 slice_reduce_fusion
  69.5 0.1 copy.45
  69.6 0.1 bitcast_exponential_fusion
  69.6 3.8 %multiply_convert_fusion = bf16[2,256,128]{2,1,0:T(8,128)(2,1)S(1)} fusion(bf16[2,256,4096]{2,1,0:T(8,128)(2,1)} %reshape.321, bf16[4096,128]{1,0:T(8,128)(2,1)} %param.21), kind=kOutput, calls=%fused_computation.57 | convolution fusion | flops 537198592 | bytes 5373952 | tf_op jit(solution)/shard_map/abf,fc->abc/dot_general | solution.py:133
  73.4 0.1 fusion.73
  73.5 0.4 fusion.27
  74.0 39.3 %custom-call.3 = f32[2,1,4,1,64,64]{4,5,3,2,1,0:T(8,128)S(1)} custom-call(f32[2,1,4,1,64,64]{5,4,3,2,1,0:T(8,128)S(1)} %fusion.27), custom_call_target="InvertDiagBlocksLowerTriangular" | custom-call | tf_op jit(solution)/shard_map/vmap(vmap())/triangular_solve | solution.py:74
  113.3 0.3 multiply_multiply_fusion
  113.6 0.6 convolution_bitcast_fusion.3
  114.2 0.1 slice_bitcast_fusion
  114.4 3.0 %while.39 = (s32[]{:T(128)}, f32[2,1,128,256]{3,2,0,1:T(8,128)S(1)}, f32[4,2,1]{1,2,0:T(1,128)S(1)}, f32[4,2,1,64,128]{4,3,0,1,2:T(8,128)S(1)}, f32[4,2,1,64,256...) while((s32[]{:T(128)}, f32[2,1,128,256]{3,2,0,1:T(8,128)S(1)}, ...), condition=%wide.region_3.4_spmd, body=%wide.region_2.3_spmd.sunk | while | flops 100827136 | bytes 1312365 | solution.py:94
  114.4 0.3 convolution_subtract_fusion.2
  114.7 0.4 fusion.110
  115.1 0.3 convolution_subtract_fusion.2
  115.4 0.4 fusion.110
  115.9 0.3 convolution_subtract_fusion.2
  116.2 0.4 fusion.110
  116.6 0.3 convolution_subtract_fusion.2
  116.9 0.4 fusion.110
  117.4 13.9 %all-gather.2 = bf16[8,1,128,128]{3,2,1,0:T(8,128)(2,1)S(1)} all-gather(bf16[2,1,128,128]{3,2,1,0:T(8,128)(2,1)S(1)} %get-tuple-element.354), channel_id=4, replica_groups=mesh['sp'=4,'tp'=8] {'sp'}, dimensions={0}, use_global_device_ids=true | all-gather | bytes 327680 | tf_op jit(solution)/shard_map/all_gather | solution.py:14
  131.4 14.6 %all-gather.1 = bf16[8,1,128,128]{3,2,1,0:T(8,128)(2,1)S(1)} all-gather(bf16[2,1,128,128]{3,2,1,0:T(8,128)(2,1)S(1)} %get-tuple-element.355), channel_id=3, replica_groups=mesh['sp'=4,'tp'=8] {'sp'}, dimensions={0}, use_global_device_ids=true | all-gather | bytes 327680 | tf_op jit(solution)/shard_map/all_gather | solution.py:14
  146.0 1.1 while.41
  146.0 0.2 fusion.116
  146.3 0.2 fusion.116
  146.6 0.2 fusion.116
  146.8 0.2 fusion.116
  147.1 16.0 %all-gather.3 = f32[8,1,128,128]{3,2,1,0:T(8,128)S(1)} all-gather(f32[2,1,128,128]{3,2,1,0:T(8,128)S(1)} %slice_bitcast_fusion.1), channel_id=5, replica_groups=mesh['sp'=4,'tp'=8] {'sp'}, dimensions={0}, use_global_device_ids=true | all-gather | bytes 655360 | tf_op jit(solution)/shard_map/all_gather | solution.py:36
  163.0 1.8 while.40
  163.1 0.4 fusion.113
  163.5 0.4 fusion.113
  164.0 0.4 fusion.113
  164.4 0.4 fusion.113
  164.8 0.3 convolution_bitcast_fusion.5
  165.1 0.2 fusion.44
  165.4 12.1 %psum.7 = f32[2,1,128]{2,0,1:T(2,128)S(1)} all-reduce(f32[2,1,128]{2,0,1:T(2,128)S(1)} %bitcast.230), channel_id=1, replica_groups=mesh['sp'=4,'tp'=8] {'sp'}, use_global_device_ids=true, to_apply=%region_11.12 | all-reduce | flops 256 | bytes 2048 | tf_op jit(solution)/shard_map/psum | solution.py:195
  177.5 1.6 multiply_reduce_fusion.1
  179.1 3.3 %convolution_bitcast_fusion.2 = f32[4096,2]{1,0:T(8,128)} fusion(bf16[128,4096]{1,0:T(8,128)(2,1)S(1)} %copy-done.2, f32[2,1,128]{2,0,1:T(2,128)S(1)} %get-tuple-element.345, f32[128]{0:T(128)S(1)} %copy-done.5, f32[2]{0:T(128)S(1)} %add_rsqrt_fusion.1, bf16[2,4096]{1,0:T(2,128)(2,1)S(1)} %copy-done.3, bf16[4096,128]{1,0:T(8,128)(2,1)} %param.23), kind=kOutput, calls=%fused_computation.29 | convolution fusion | flops 4196352 | bytes 2147848
  182.4 0.0 reduce-scatter.4.cloned.1.call-update
  182.4 0.9 fusion.30
  183.3 37.6 %reduce-scatter.4.cloned.1.call-done = f32[512,2]{1,0:T(8,128)} async-done(((f32[4096,2]{1,0:T(8,128)}), f32[512,2]{1,0:T(8,128)}) %reduce-scatter.4.cloned.1.call-update) | async-done | bytes 4112
  220.9 1.6 copy.63
  (36 shorter events, 0.3 us)
Async XLA Ops:
  7.2 4.4 %copy-start = (bf16[4096,128]{1,0:T(8,128)(2,1)S(1)}, bf16[4096,128]{1,0:T(8,128)(2,1)}, u32[]{:S(2)}) copy-start(bf16[4096,128]{1,0:T(8,128)(2,1)} %param.20) | copy-start | bytes 3145732
  7.2 42.0 %all-gather.6.cloned.1.call-start = ((), (), s32[]{:S(2)}) async-start(), calls=%async_computation.1 | async-start | bytes 4718592 | tf_op jit(solution)/shard_map/all_gather | solution.py:118
  7.9 213.0 %reduce-scatter.4.cloned.1.call-start = ((), (), s32[]{:S(2)}) async-start(), calls=%async_computation.2 | async-start | bytes 2359296
  63.1 3.5 %copy-start.1 = (bf16[2,256,4096]{2,1,0:T(8,128)(2,1)S(1)}, bf16[2,256,4096]{2,1,0:T(8,128)(2,1)}, u32[]{:S(2)}) copy-start(bf16[2,256,4096]{2,1,0:T(8,128)(2,1)} %reshape.321) | copy-start | bytes 12582916
  66.7 1.4 copy-start.4
  131.3 46.2 %copy-start.3 = (bf16[2,4096]{1,0:T(2,128)(2,1)S(1)}, bf16[2,4096]{1,0:T(2,128)(2,1)}, u32[]{:S(2)}) copy-start(bf16[2,4096]{1,0:T(2,128)(2,1)} %param.19) | copy-start | bytes 49156
  146.0 33.1 %copy-start.2 = (bf16[128,4096]{1,0:T(8,128)(2,1)S(1)}, bf16[128,4096]{1,0:T(8,128)(2,1)}, u32[]{:S(2)}) copy-start(bf16[128,4096]{1,0:T(8,128)(2,1)} %param.29) | copy-start | bytes 3145732
  146.0 33.1 %copy-start.5 = (f32[128]{0:T(128)S(1)}, f32[128]{0:T(128)}, u32[]{:S(2)}) copy-start(f32[128]{0:T(128)} %param.28) | copy-start | bytes 1540
Sparse Core Ops, SparseCore 0:
  9.9 39.2 all-gather.5
  182.6 38.3 reduce-scatter.3
